TPU v7x, 32 devices: a whole 2x2x4 slice. The times are simulated.
32 devices in a mesh: tp: 8 (over z, y), dp: 4 (over x, core).
Axes of the slice: x: 2, y: 2, z: 4, core: 2. Of those that a mesh axis runs over, the one named last changes fastest.
Arguments:
- tokens: bfloat16 [128, 4096], P('dp', 'tp'), may hold values from -6 to 6
- lengths: int32 [128], P('dp'), may hold values from 1 to 96, 3072 in all
- norm_gain: float32 [2, 4096], replicated, may hold values from 0.1 to 1.9
- w_recept: bfloat16 [2, 4096, 4096], P(None, None, ('tp', 'dp')), may hold values from -0.09375 to 0.09375
- w_key: bfloat16 [2, 4096, 4096], P(None, None, ('tp', 'dp')), may hold values from -0.09375 to 0.09375
- w_value: bfloat16 [2, 4096, 4096], P(None, None, ('tp', 'dp')), may hold values from -0.09375 to 0.09375
- w_decay: bfloat16 [2, 4096, 4096], P(None, None, ('tp', 'dp')), may hold values from -0.09375 to 0.09375
- w_rate: bfloat16 [2, 4096, 4096], P(None, None, ('tp', 'dp')), may hold values from -0.09375 to 0.09375
- w_gate: bfloat16 [2, 4096, 4096], P(None, None, ('tp', 'dp')), may hold values from -0.09375 to 0.09375
- w_out: bfloat16 [2, 4096, 4096], P(None, None, ('tp', 'dp')), may hold values from -0.09375 to 0.09375
- decay_base: float32 [2, 4096], P(None, 'tp'), may hold values from -3 to 1
- rate_base: float32 [2, 4096], P(None, 'tp'), may hold values from -3 to 3
- group_gain: float32 [2, 4096], P(None, 'tp'), may hold values from 0.1 to 1.9
- state: float32 [2, 128, 64, 64, 64], P(None, 'dp', 'tp'), may hold values from -6 to 6
Outputs:
- mixed: bfloat16 [128, 4096], P('dp', 'tp')
- new_state: float32 [2, 128, 64, 64, 64], P(None, 'dp', 'tp')
Inputs may be any that keep to these rules, and one draw needn't show every extreme that they name: Each sequence's live length lies between 1 and 96, some sequences reach 96, and the lengths sum to 3072.
All inputs are finite; a program needn't handle non-finite values.
Results may differ from a plain program's by a relative error of at most 0.025.
Values may be sent and summed in bfloat16 or wider, within the bound.
A program may use at most 128 MiB of HBM per device.

v0:
```python
import jax
import jax.numpy as jnp
from jax import lax
from jax.sharding import PartitionSpec as P

STEP = 16
RMS_EPS = 1e-06
GROUP_EPS = 0.00064


def as_sent(value):

    def short(part):
        return part.astype(jnp.bfloat16) if part.dtype == jnp.float32 else part

    return jax.tree.map(short, value)


def taken_in(section, axis, dim, hop, start):

    def gathered(part):
        return lax.all_gather(part, axis, axis=dim, tiled=True)

    return hop(start, jax.tree.map(gathered, section), jnp.int32(0))


def recur(state_old, recept, key_vec, value_vec, decay_rate, learn_rate, active, head_size):
    split = (recept.shape[0], -1, head_size)
    recept_h = recept.reshape(split)
    key_h = key_vec.reshape(split)
    value_h = value_vec.reshape(split)
    decay_h = decay_rate.reshape(split)
    rate_h = learn_rate.reshape(split)
    key_len = jnp.sqrt(jnp.sum(key_h * key_h, axis=-1, keepdims=True))
    key_unit = key_h / jnp.maximum(key_len, 1e-12)
    state_a = jnp.einsum("bhij,bhj->bhi", state_old, -key_unit, precision=lax.Precision.HIGHEST)
    updated = (
        state_old * decay_h[:, :, None, :]
        + state_a[:, :, :, None] * (key_unit * rate_h)[:, :, None, :]
        + value_h[:, :, :, None] * (key_h * rate_h)[:, :, None, :]
    )
    updated = jnp.where(active[:, None, None, None], updated, state_old)
    readout = jnp.einsum("bhij,bhj->bhi", updated, recept_h, precision=lax.Precision.HIGHEST)
    centre = jnp.mean(readout, axis=-1, keepdims=True)
    spread = jnp.mean(jnp.square(readout - centre), axis=-1, keepdims=True)
    normal_out = ((readout - centre) * lax.rsqrt(spread + GROUP_EPS)).reshape(recept.shape[0], -1)
    return (updated, normal_out)


def on_device(
    tokens,
    lengths,
    norm_gain,
    w_recept,
    w_key,
    w_value,
    w_decay,
    w_rate,
    w_gate,
    w_out,
    decay_base,
    rate_base,
    group_gain,
    state,
):
    slim = w_recept.shape[2]
    head_size = state.shape[-1]
    active = lengths > STEP
    current = tokens
    updated_states = []
    for layer_idx in range(2):
        joined = jnp.concatenate(
            [
                w_recept[layer_idx],
                w_key[layer_idx],
                w_value[layer_idx],
                w_decay[layer_idx],
                w_rate[layer_idx],
                w_gate[layer_idx],
            ],
            axis=1,
        )
        batch_raw = lax.all_gather(current, "dp", axis=0, tiled=True)
        every_feature = lax.all_gather(batch_raw, "tp", axis=1, tiled=True)
        values = every_feature.astype(jnp.float32)
        factor = lax.rsqrt(jnp.mean(values * values, axis=1, keepdims=True) + RMS_EPS)
        normed = (values * factor * norm_gain[layer_idx]).astype(jnp.bfloat16)
        projected = jnp.dot(normed, joined, preferred_element_type=jnp.float32)
        pieces = [
            projected[:, idx * slim : (idx + 1) * slim].astype(jnp.bfloat16) for idx in range(6)
        ]
        arrived = (
            lax.all_to_all(as_sent(pieces[0]), "dp", split_axis=0, concat_axis=1, tiled=True),
            lax.all_to_all(as_sent(pieces[1]), "dp", split_axis=0, concat_axis=1, tiled=True),
            lax.all_to_all(as_sent(pieces[2]), "dp", split_axis=0, concat_axis=1, tiled=True),
            lax.all_to_all(as_sent(pieces[3]), "dp", split_axis=0, concat_axis=1, tiled=True),
            lax.all_to_all(as_sent(pieces[4]), "dp", split_axis=0, concat_axis=1, tiled=True),
            lax.all_to_all(as_sent(pieces[5]), "dp", split_axis=0, concat_axis=1, tiled=True),
        )
        recept, key_vec, value_vec, decay_pre, rate_pre, gate_pre = [
            item.astype(jnp.float32) for item in arrived
        ]
        decay_rate = jnp.exp(-jnp.exp(-jax.nn.softplus(-(decay_base[layer_idx] + decay_pre)) - 0.5))
        learn_rate = jax.nn.sigmoid(rate_base[layer_idx] + rate_pre)
        gate_open = jax.nn.sigmoid(gate_pre)
        updated, normal_out = recur(
            state[layer_idx], recept, key_vec, value_vec, decay_rate, learn_rate, active, head_size
        )
        updated_states.append(updated)
        mixed_here = jnp.where(
            active[:, None], normal_out * group_gain[layer_idx] * gate_open, 0.0
        ).astype(jnp.bfloat16)
        rows_all = lax.all_gather(mixed_here, "dp", axis=0, tiled=True)
        out_weight = w_out[layer_idx]

        def fold_output(acc_sum, segment, offset):
            weight_rows = lax.dynamic_slice_in_dim(out_weight, offset, segment.shape[1], 0)
            return acc_sum + jnp.dot(segment, weight_rows, preferred_element_type=jnp.float32)

        blank = jnp.zeros((rows_all.shape[0], out_weight.shape[1]), jnp.float32)
        out_cols = taken_in(rows_all, "tp", 1, fold_output, blank).astype(jnp.bfloat16)
        current = lax.all_to_all(out_cols, "dp", split_axis=0, concat_axis=1, tiled=True)
    return (current, jnp.stack(updated_states))


def solution(mesh):
    in_specs = (
        P("dp", "tp"),
        P("dp"),
        P(),
        P(None, None, ("tp", "dp")),
        P(None, None, ("tp", "dp")),
        P(None, None, ("tp", "dp")),
        P(None, None, ("tp", "dp")),
        P(None, None, ("tp", "dp")),
        P(None, None, ("tp", "dp")),
        P(None, None, ("tp", "dp")),
        P(None, "tp"),
        P(None, "tp"),
        P(None, "tp"),
        P(None, "dp", "tp", None, None),
    )
    out_specs = (P("dp", "tp"), P(None, "dp", "tp", None, None))
    return jax.shard_map(
        on_device, mesh=mesh, in_specs=in_specs, out_specs=out_specs, check_vma=False
    )
```

profile of v0, /device:TPU:0, one launch (start us, length us, event | category | flops | bytes accessed | tf_op | source)
XLA Modules:
  0.0 369.8 jit_solution(15429060833024685349)
XLA Ops:
  7.2 8.5 %all_gather.24 = bf16[128,512]{1,0:T(8,128)(2,1)} all-gather(bf16[32,512]{1,0:T(8,128)(2,1)} %param.14), channel_id=1, replica_groups=mesh['tp'=8,'dp'=4] {'dp'}, dimensions={0}, use_global_device_ids=true | all-gather | bytes 163840 | tf_op jit(solution)/shard_map/all_gather | solution.py:83
  29.2 26.5 %all-gather.5.cloned.1.call-done = bf16[128,4096]{1,0:T(8,128)(2,1)} async-done(((bf16[128,512]{1,0:T(8,128)(2,1)}), bf16[128,4096]{1,0:T(8,128)(2,1)}) %all-gather.5.cloned.1.call-update) | async-done | bytes 1048592 | tf_op jit(solution)/shard_map/all_gather | solution.py:84
  57.3 4.2 %convolution_convert_fusion.1 = bf16[128,768]{1,0:T(8,128)(2,1)S(1)} fusion(bf16[4096,768]{1,0:T(8,128)(2,1)} %get-tuple-element.8, bf16[128,4096]{1,0:T(8,128)(2,1)} %all-gather.5.cloned.1.call-done, f32[4096]{0:T(1024)S(1)} %bitcast.161, f32[128]{0:T(128)S(1)} %add_rsqrt_fusion.3), kind=kOutput, calls=%fused_computation.48 | convolution fusion | flops 807501824 | bytes 7553536 | tf_op jit(solution)/shard_map/dot_general | solution.py:88
  65.4 3.9 %all-to-all-done.4 = bf16[4,32,128]{2,1,0:T(8,128)(2,1)S(1)} async-done(((bf16[4,32,128]{2,1,0:T(8,128)(2,1)}), bf16[4,32,128]{2,1,0:T(8,128)(2,1)S(1)}, u32[]{:S(2)}, u32[]{:S(2)}) %all-to-all-start.4) | async-done | bytes 32800 | tf_op jit(solution)/shard_map/all_to_all | solution.py:93
  79.8 3.9 %all-to-all-done.2 = bf16[4,32,128]{2,1,0:T(8,128)(2,1)S(1)} async-done(((bf16[4,32,128]{2,1,0:T(8,128)(2,1)}), bf16[4,32,128]{2,1,0:T(8,128)(2,1)S(1)}, u32[]{:S(2)}, u32[]{:S(2)}) %all-to-all-start.2) | async-done | bytes 32800 | tf_op jit(solution)/shard_map/all_to_all | solution.py:97
  86.9 3.9 %all-to-all-done.3 = bf16[4,32,128]{2,1,0:T(8,128)(2,1)S(1)} async-done(((bf16[4,32,128]{2,1,0:T(8,128)(2,1)}), bf16[4,32,128]{2,1,0:T(8,128)(2,1)S(1)}, u32[]{:S(2)}, u32[]{:S(2)}) %all-to-all-start.3) | async-done | bytes 32800 | tf_op jit(solution)/shard_map/all_to_all | solution.py:95
  102.3 15.4 %fusion = f32[32,8,1,64]{3,2,1,0:T(1,128)S(1)} fusion(f32[32,8,64,1]{2,3,1,0:T(1,128)S(1)} %bitcast.154, f32[2,32,8,64,64]{4,3,2,1,0:T(8,128)} %param.27), kind=kOutput, calls=%fused_computation.2 | convolution fusion | flops 12582912 | bytes 8519680 | tf_op jit(solution)/shard_map/bhij,bhj->bhi/dot_general | solution.py:36
  117.7 11.1 %fusion.4 = f32[32,8,1,64]{3,2,1,0:T(1,128)S(1)} fusion(bf16[32,8,64,1]{2,3,1,0:T(2,128)(2,1)S(1)} %reshape.317, f32[2,32,8,64,64]{4,3,2,1,0:T(8,128)} %param.27, f32[32,8,64]{2,1,0:T(8,128)S(1)} %get-tuple-element.23, f32[32,8,64]{2,1,0:T(8,128)S(1)} %reshape.299, f32[32,8,64]{2,1,0:T(8,128)S(1)} %get-tuple-element.22, f32[32,8,64]{2,1,0:T(8,128)S(1)} %bitcast.150, ...), kind=kOutput, calls=%fused_computation.7 | convolution fusion | flops 18874368 | bytes 8814624 | tf_op jit(solution)/shard_map/bhij,bhj->bhi/dot_general | solution.py:43
  129.4 6.1 %all_gather.26 = bf16[128,512]{1,0:T(8,128)(2,1)} all-gather(bf16[32,512]{1,0:T(8,128)(2,1)S(1)} %fusion.59), channel_id=1, replica_groups=mesh['tp'=8,'dp'=4] {'dp'}, dimensions={0}, use_global_device_ids=true | all-gather | bytes 163840 | tf_op jit(solution)/shard_map/all_gather | solution.py:113
  135.5 38.9 %all-gather.7.cloned.1.call-done = bf16[128,4096]{1,0:T(8,128)(2,1)} async-done(((bf16[128,512]{1,0:T(8,128)(2,1)}), bf16[128,4096]{1,0:T(8,128)(2,1)}) %all-gather.7.cloned.1.call-update) | async-done | bytes 1048592 | tf_op jit(solution)/shard_map/all_gather | solution.py:22
  176.4 6.6 %all_to_all.200 = bf16[4,32,128]{2,1,0:T(8,128)(2,1)S(1)} all-to-all(bf16[4,32,128]{2,1,0:T(8,128)(2,1)S(1)} %bitcast.159), channel_id=1, replica_groups=mesh['tp'=8,'dp'=4] {'dp'}, dimensions={0} | all-to-all | bytes 65536 | tf_op jit(solution)/shard_map/all_to_all | solution.py:122
  183.0 5.9 %all_gather.28 = bf16[128,512]{1,0:T(8,128)(2,1)} all-gather(bf16[32,512]{1,0:T(8,128)(2,1)S(1)} %copy_bitcast_fusion.1), channel_id=1, replica_groups=mesh['tp'=8,'dp'=4] {'dp'}, dimensions={0}, use_global_device_ids=true | all-gather | bytes 163840 | tf_op jit(solution)/shard_map/all_gather | solution.py:83
  188.9 37.5 %all-gather.9.cloned.1.call-done = bf16[128,4096]{1,0:T(8,128)(2,1)} async-done(((bf16[128,512]{1,0:T(8,128)(2,1)}), bf16[128,4096]{1,0:T(8,128)(2,1)}) %all-gather.9.cloned.1.call-update) | async-done | bytes 1048592 | tf_op jit(solution)/shard_map/all_gather | solution.py:84
  228.0 4.2 %convolution_convert_fusion = bf16[128,768]{1,0:T(8,128)(2,1)S(1)} fusion(bf16[4096,768]{1,0:T(8,128)(2,1)} %get-tuple-element.9, bf16[128,4096]{1,0:T(8,128)(2,1)} %all-gather.9.cloned.1.call-done, f32[4096]{0:T(1024)S(1)} %bitcast.160, f32[128]{0:T(128)S(1)} %add_rsqrt_fusion.2), kind=kOutput, calls=%fused_computation.47 | convolution fusion | flops 807501824 | bytes 7553536 | tf_op jit(solution)/shard_map/dot_general | solution.py:88
  232.8 6.6 %all_to_all.201 = bf16[4,32,128]{2,1,0:T(8,128)(2,1)S(1)} all-to-all(bf16[4,32,128]{2,1,0:T(8,128)(2,1)S(1)} %bitcast.156), channel_id=1, replica_groups=mesh['tp'=8,'dp'=4] {'dp'}, dimensions={0} | all-to-all | bytes 65536 | tf_op jit(solution)/shard_map/all_to_all | solution.py:93
  242.8 3.8 %all-to-all-done.8 = bf16[4,32,128]{2,1,0:T(8,128)(2,1)S(1)} async-done(((bf16[4,32,128]{2,1,0:T(8,128)(2,1)}), bf16[4,32,128]{2,1,0:T(8,128)(2,1)S(1)}, u32[]{:S(2)}, u32[]{:S(2)}) %all-to-all-start.8) | async-done | bytes 32800 | tf_op jit(solution)/shard_map/all_to_all | solution.py:94
  249.9 3.9 %all-to-all-done.9 = bf16[4,32,128]{2,1,0:T(8,128)(2,1)S(1)} async-done(((bf16[4,32,128]{2,1,0:T(8,128)(2,1)}), bf16[4,32,128]{2,1,0:T(8,128)(2,1)S(1)}, u32[]{:S(2)}, u32[]{:S(2)}) %all-to-all-start.9) | async-done | bytes 32800 | tf_op jit(solution)/shard_map/all_to_all | solution.py:97
  257.1 3.9 %all-to-all-done.10 = bf16[4,32,128]{2,1,0:T(8,128)(2,1)S(1)} async-done(((bf16[4,32,128]{2,1,0:T(8,128)(2,1)}), bf16[4,32,128]{2,1,0:T(8,128)(2,1)S(1)}, u32[]{:S(2)}, u32[]{:S(2)}) %all-to-all-start.10) | async-done | bytes 32800 | tf_op jit(solution)/shard_map/all_to_all | solution.py:95
  272.3 15.4 %fusion.5 = f32[32,8,1,64]{3,2,1,0:T(1,128)S(1)} fusion(f32[32,8,64,1]{2,3,1,0:T(1,128)S(1)} %bitcast.155, f32[2,32,8,64,64]{4,3,2,1,0:T(8,128)} %param.27), kind=kOutput, calls=%fused_computation.9 | convolution fusion | flops 12582912 | bytes 8519680 | tf_op jit(solution)/shard_map/bhij,bhj->bhi/dot_general | solution.py:36
  287.8 11.1 %fusion.9 = f32[32,8,1,64]{3,2,1,0:T(1,128)S(1)} fusion(bf16[32,8,64,1]{2,3,1,0:T(2,128)(2,1)S(1)} %reshape.319, f32[2,32,8,64,64]{4,3,2,1,0:T(8,128)} %param.27, f32[32,8,64]{2,1,0:T(8,128)S(1)} %get-tuple-element.21, f32[32,8,64]{2,1,0:T(8,128)S(1)} %reshape.305, f32[32,8,64]{2,1,0:T(8,128)S(1)} %get-tuple-element.20, f32[32,8,64]{2,1,0:T(8,128)S(1)} %bitcast.152, ...), kind=kOutput, calls=%fused_computation.14 | convolution fusion | flops 18874368 | bytes 8814624 | tf_op jit(solution)/shard_map/bhij,bhj->bhi/dot_general | solution.py:43
  299.5 5.9 %all_gather.30 = bf16[128,512]{1,0:T(8,128)(2,1)} all-gather(bf16[32,512]{1,0:T(8,128)(2,1)S(1)} %fusion.57), channel_id=1, replica_groups=mesh['tp'=8,'dp'=4] {'dp'}, dimensions={0}, use_global_device_ids=true | all-gather | bytes 163840 | tf_op jit(solution)/shard_map/all_gather | solution.py:113
  305.4 13.7 %add_select_fusion.1 = (f32[1,32,8,64,64]{4,3,2,1,0:T(8,128)}, f32[1,32,8,64,64]{4,3,2,1,0:T(8,128)}) fusion(f32[2,32,8,64,64]{4,3,2,1,0:T(8,128)} %param.27, f32[32,8,64]{2,1,0:T(8,128)S(1)} %get-tuple-element.23, f32[32,8,64]{2,1,0:T(8,128)S(1)} %reshape.299, f32[32,8,64]{2,1,0:T(8,128)S(1)} %get-tuple-element.22, f32[32,8,64]{2,1,0:T(8,128)S(1)} %bitcast.151, ...), kind=kLoop, calls=%fused_computation.16 | loop fusion | flops 12582912 | bytes 17432608 | tf_op jit(solution)/shard_map/jit(_where)/select_n | solution.py:42
  319.1 25.2 %all-gather.11.cloned.1.call-done = bf16[128,4096]{1,0:T(8,128)(2,1)} async-done(((bf16[128,512]{1,0:T(8,128)(2,1)}), bf16[128,4096]{1,0:T(8,128)(2,1)}) %all-gather.11.cloned.1.call-update) | async-done | bytes 1048592 | tf_op jit(solution)/shard_map/all_gather | solution.py:22
  350.2 12.5 %pad_maximum_fusion = f32[2,32,8,64,64]{4,3,2,1,0:T(8,128)} fusion(f32[1,32,8,64,64]{4,3,2,1,0:T(8,128)} %get-tuple-element.7, f32[1,32,8,64,64]{4,3,2,1,0:T(8,128)} %get-tuple-element.6), kind=kLoop, calls=%fused_computation | loop fusion | flops 2097152 | bytes 16777216 | tf_op jit(solution)/shard_map/stack | solution.py:123
  (116 shorter events, 77.2 us)
Async XLA Ops:
  7.2 15.8 %copy-start = (bf16[2,4096,128]{2,1,0:T(8,128)(2,1)S(1)}, bf16[2,4096,128]{2,1,0:T(8,128)(2,1)}, u32[]{:S(2)}) copy-start(bf16[2,4096,128]{2,1,0:T(8,128)(2,1)} %param.19) | copy-start | bytes 6291460
  7.2 48.6 %all-gather.5.cloned.1.call-start = ((), (), s32[]{:S(2)}) async-start(), calls=%async_computation.14 | async-start | bytes 1179648 | tf_op jit(solution)/shard_map/all_gather | solution.py:84
  16.5 8.0 %copy-start.1 = (bf16[2,4096,128]{2,1,0:T(8,128)(2,1)S(1)}, bf16[2,4096,128]{2,1,0:T(8,128)(2,1)}, u32[]{:S(2)}) copy-start(bf16[2,4096,128]{2,1,0:T(8,128)(2,1)} %param.20) | copy-start | bytes 6291460
  19.7 6.3 %copy-start.2 = (bf16[2,4096,128]{2,1,0:T(8,128)(2,1)S(1)}, bf16[2,4096,128]{2,1,0:T(8,128)(2,1)}, u32[]{:S(2)}) copy-start(bf16[2,4096,128]{2,1,0:T(8,128)(2,1)} %param.21) | copy-start | bytes 6291460
  23.0 4.6 %copy-start.4 = (f32[2,4096]{1,0:T(2,128)S(1)}, f32[2,4096]{1,0:T(2,128)}, u32[]{:S(2)}) copy-start(f32[2,4096]{1,0:T(2,128)} %param.16) | copy-start | bytes 98308
  23.0 4.6 %copy-start.3 = (bf16[2,4096,128]{2,1,0:T(8,128)(2,1)S(1)}, bf16[2,4096,128]{2,1,0:T(8,128)(2,1)}, u32[]{:S(2)}) copy-start(bf16[2,4096,128]{2,1,0:T(8,128)(2,1)} %param.22) | copy-start | bytes 6291460
  27.6 37.8 %copy-start.7 = (s32[32]{0:T(128)S(1)}, s32[32]{0:T(128)}, u32[]{:S(2)}) copy-start(s32[32]{0:T(128)} %param.15) | copy-start | bytes 388
  27.6 44.9 %copy-start.5 = (f32[2,512]{1,0:T(2,128)S(1)}, f32[2,512]{1,0:T(2,128)}, u32[]{:S(2)}) copy-start(f32[2,512]{1,0:T(2,128)} %param.25) | copy-start | bytes 12292
  27.6 44.9 %copy-start.6 = (f32[2,512]{1,0:T(2,128)S(1)}, f32[2,512]{1,0:T(2,128)}, u32[]{:S(2)}) copy-start(f32[2,512]{1,0:T(2,128)} %param.24) | copy-start | bytes 12292
  62.1 7.2 %all-to-all-start.4 = ((bf16[4,32,128]{2,1,0:T(8,128)(2,1)}), bf16[4,32,128]{2,1,0:T(8,128)(2,1)S(1)}, u32[]{:S(2)}, u32[]{:S(2)}) async-start(bf16[4,32,128]{2,1,0:T(8,128)(2,1)} %bitcast.21), calls=%async_computation.4 | async-start | bytes 65536 | tf_op jit(solution)/shard_map/all_to_all | solution.py:93
  69.3 7.2 %all-to-all-start.1 = ((bf16[4,32,128]{2,1,0:T(8,128)(2,1)}), bf16[4,32,128]{2,1,0:T(8,128)(2,1)S(1)}, u32[]{:S(2)}, u32[]{:S(2)}) async-start(bf16[4,32,128]{2,1,0:T(8,128)(2,1)} %bitcast.11), calls=%async_computation.1 | async-start | bytes 65536 | tf_op jit(solution)/shard_map/all_to_all | solution.py:94
  76.5 7.2 %all-to-all-start.2 = ((bf16[4,32,128]{2,1,0:T(8,128)(2,1)}), bf16[4,32,128]{2,1,0:T(8,128)(2,1)S(1)}, u32[]{:S(2)}, u32[]{:S(2)}) async-start(bf16[4,32,128]{2,1,0:T(8,128)(2,1)} %bitcast.17), calls=%async_computation.2 | async-start | bytes 65536 | tf_op jit(solution)/shard_map/all_to_all | solution.py:97
  83.6 7.2 %all-to-all-start.3 = ((bf16[4,32,128]{2,1,0:T(8,128)(2,1)}), bf16[4,32,128]{2,1,0:T(8,128)(2,1)S(1)}, u32[]{:S(2)}, u32[]{:S(2)}) async-start(bf16[4,32,128]{2,1,0:T(8,128)(2,1)} %bitcast.19), calls=%async_computation.3 | async-start | bytes 65536 | tf_op jit(solution)/shard_map/all_to_all | solution.py:95
  90.8 7.2 %all-to-all-start = ((bf16[4,32,128]{2,1,0:T(8,128)(2,1)}), bf16[4,32,128]{2,1,0:T(8,128)(2,1)S(1)}, u32[]{:S(2)}, u32[]{:S(2)}) async-start(bf16[4,32,128]{2,1,0:T(8,128)(2,1)} %bitcast.9), calls=%async_computation | async-start | bytes 65536 | tf_op jit(solution)/shard_map/all_to_all | solution.py:96
  98.0 31.3 %all-to-all-start.5 = ((bf16[4,32,128]{2,1,0:T(8,128)(2,1)}), bf16[4,32,128]{2,1,0:T(8,128)(2,1)S(1)}, u32[]{:S(2)}, u32[]{:S(2)}) async-start(bf16[4,32,128]{2,1,0:T(8,128)(2,1)} %bitcast.26), calls=%async_computation.5 | async-start | bytes 65536 | tf_op jit(solution)/shard_map/all_to_all | solution.py:98
  101.3 73.2 %all-gather.7.cloned.1.call-start = ((), (), s32[]{:S(2)}) async-start(), calls=%async_computation.15 | async-start | bytes 1179648 | tf_op jit(solution)/shard_map/all_gather | solution.py:22
  135.5 91.0 %all-gather.9.cloned.1.call-start = ((), (), s32[]{:S(2)}) async-start(), calls=%async_computation.16 | async-start | bytes 1179648 | tf_op jit(solution)/shard_map/all_gather | solution.py:84
  239.4 7.2 %all-to-all-start.8 = ((bf16[4,32,128]{2,1,0:T(8,128)(2,1)}), bf16[4,32,128]{2,1,0:T(8,128)(2,1)S(1)}, u32[]{:S(2)}, u32[]{:S(2)}) async-start(bf16[4,32,128]{2,1,0:T(8,128)(2,1)} %bitcast.40), calls=%async_computation.8 | async-start | bytes 65536 | tf_op jit(solution)/shard_map/all_to_all | solution.py:94
  246.6 7.2 %all-to-all-start.9 = ((bf16[4,32,128]{2,1,0:T(8,128)(2,1)}), bf16[4,32,128]{2,1,0:T(8,128)(2,1)S(1)}, u32[]{:S(2)}, u32[]{:S(2)}) async-start(bf16[4,32,128]{2,1,0:T(8,128)(2,1)} %bitcast.46), calls=%async_computation.9 | async-start | bytes 65536 | tf_op jit(solution)/shard_map/all_to_all | solution.py:97
  253.8 7.2 %all-to-all-start.10 = ((bf16[4,32,128]{2,1,0:T(8,128)(2,1)}), bf16[4,32,128]{2,1,0:T(8,128)(2,1)S(1)}, u32[]{:S(2)}, u32[]{:S(2)}) async-start(bf16[4,32,128]{2,1,0:T(8,128)(2,1)} %bitcast.48), calls=%async_computation.10 | async-start | bytes 65536 | tf_op jit(solution)/shard_map/all_to_all | solution.py:95
  261.0 7.2 %all-to-all-start.7 = ((bf16[4,32,128]{2,1,0:T(8,128)(2,1)}), bf16[4,32,128]{2,1,0:T(8,128)(2,1)S(1)}, u32[]{:S(2)}, u32[]{:S(2)}) async-start(bf16[4,32,128]{2,1,0:T(8,128)(2,1)} %bitcast.38), calls=%async_computation.7 | async-start | bytes 65536 | tf_op jit(solution)/shard_map/all_to_all | solution.py:96
  268.1 31.3 %all-to-all-start.12 = ((bf16[4,32,128]{2,1,0:T(8,128)(2,1)}), bf16[4,32,128]{2,1,0:T(8,128)(2,1)S(1)}, u32[]{:S(2)}, u32[]{:S(2)}) async-start(bf16[4,32,128]{2,1,0:T(8,128)(2,1)} %bitcast.55), calls=%async_computation.12 | async-start | bytes 65536 | tf_op jit(solution)/shard_map/all_to_all | solution.py:98
  271.4 72.9 %all-gather.11.cloned.1.call-start = ((), (), s32[]{:S(2)}) async-start(), calls=%async_computation.17 | async-start | bytes 1179648 | tf_op jit(solution)/shard_map/all_gather | solution.py:22
  346.9 15.8 %all-to-all-start.13 = ((bf16[4,32,128]{2,1,0:T(8,128)(2,1)}), bf16[4,32,128]{2,1,0:T(8,128)(2,1)S(1)}, u32[]{:S(2)}, u32[]{:S(2)}) async-start(bf16[4,32,128]{2,1,0:T(8,128)(2,1)} %bitcast.58), calls=%async_computation.13 | async-start | bytes 65536 | tf_op jit(solution)/shard_map/all_to_all | solution.py:122
Sparse Core Ops, SparseCore 0:
  15.9 39.8 all-gather.4
  135.6 38.8 all-gather.6
  189.0 37.3 all-gather.8
  305.6 38.7 all-gather.10
where the time goes:
time: 371 us; the launch traced here: 370 us
  waiting for transfers between devices  163 us (44%)
  matrix products  65.7 us (18%)
  blocking collectives  39.6 us (11%)
  starting transfers between devices  39.3 us (11%)
  other arithmetic  31 us (8%)
  local copies, waits for them, and re-layouts  17.3 us (5%)
  between operations  14.3 us (4%)
    all_gather x2, waiting for transfers between devices, gathered(): return lax.all_gather(part, axis, axis=dim, tiled=True)  64.1 us
    all_gather x2, waiting for transfers between devices, on_device(): every_feature = lax.all_gather(batch_raw, 'tp', axis=1, tiled=True)  64.1 us
    dot_general x2, matrix products, recur(): jnp.einsum('bhij,bhj->bhi', state_old, -key_unit, precision=lax.Precision...  30.8 us
    dot_general x2, matrix products, recur(): jnp.einsum('bhij,bhj->bhi', updated, recept_h, precision=lax.Precision.HI...  22.1 us
    all_gather x2, blocking collectives, on_device(): batch_raw = lax.all_gather(current, 'dp', axis=0, tiled=True)  14.4 us
    select_n x1, other arithmetic, recur(): updated = jnp.where(active[:, None, None, None], updated, state_old)  13.7 us
    another operation x1, other arithmetic, on_device(): return (current, jnp.stack(updated_states))  12.5 us
    all_gather x2, blocking collectives, on_device(): rows_all = lax.all_gather(mixed_here, 'dp', axis=0, tiled=True)  12 us
  transfers between devices with their start and end apart: 16, of which 13 were waited for; matrix products, arithmetic and copies ran while one was open for 26% of the time, Pallas kernels for 0%

commit v1 on v0

--- a/solution.py
+++ b/solution.py
@@ -81,7 +81,14 @@
             axis=1,
         )
         batch_raw = lax.all_gather(current, "dp", axis=0, tiled=True)
-        every_feature = lax.all_gather(batch_raw, "tp", axis=1, tiled=True)
+        ring = [batch_raw]
+        for hop_ in range(7):
+            ring.append(lax.ppermute(ring[-1], "tp", [(dev, (dev + 1) % 8) for dev in range(8)]))
+        every_feature = jnp.roll(
+            jnp.concatenate(ring[::-1], axis=1),
+            (lax.axis_index("tp") + 1) * ring[0].shape[1],
+            axis=1,
+        )
         values = every_feature.astype(jnp.float32)
         factor = lax.rsqrt(jnp.mean(values * values, axis=1, keepdims=True) + RMS_EPS)
         normed = (values * factor * norm_gain[layer_idx]).astype(jnp.bfloat16)

time: 371 us -> 397 us (1.070)
  waiting for transfers between devices: 163 us -> 194 us
  local copies, waits for them, and re-layouts: 17.3 us -> 12.8 us
    ppermute x0 -> x14, waiting for transfers between devices: none -> 99.2 us  [on_device(): lax.ppermute(ring[-1], 'tp', [(dev, (dev + 1) % 8) for dev in range(8)])]
    all_gather x2 -> x0, waiting for transfers between devices: 64.1 us -> none  [on_device(): every_feature = lax.all_gather(batch_raw, 'tp', axis=1, tiled=True)]
    unnamed x21 -> x41, local copies, waits for them, and re-layouts: 11.1 us -> 8.4 us
  transfers between devices with their start and end apart: 16 -> 28, of which waited for: 13 -> 25; matrix products, arithmetic and copies ran while one was open for 26% -> 22% of each run, Pallas kernels for 0% -> 0%
where the time goes in v1:
time: 397 us; the launch traced here: 396 us
  waiting for transfers between devices  194 us (49%)
  matrix products  65.7 us (17%)
  starting transfers between devices  42.5 us (11%)
  blocking collectives  36.9 us (9%)
  other arithmetic  29.3 us (7%)
  between operations  14.8 us (4%)
  local copies, waits for them, and re-layouts  12.8 us (3%)
    ppermute x14, waiting for transfers between devices, on_device(): lax.ppermute(ring[-1], 'tp', [(dev, (dev + 1) % 8) for dev in range(8)])  99.2 us
    all_gather x2, waiting for transfers between devices, gathered(): return lax.all_gather(part, axis, axis=dim, tiled=True)  60.6 us
    dot_general x2, matrix products, recur(): jnp.einsum('bhij,bhj->bhi', state_old, -key_unit, precision=lax.Precision...  30.8 us
    dot_general x2, matrix products, recur(): jnp.einsum('bhij,bhj->bhi', updated, recept_h, precision=lax.Precision.HI...  22.1 us
    select_n x1, other arithmetic, recur(): updated = jnp.where(active[:, None, None, None], updated, state_old)  13.7 us
    another operation x1, other arithmetic, on_device(): return (current, jnp.stack(updated_states))  12.5 us
    all_gather x2, blocking collectives, on_device(): batch_raw = lax.all_gather(current, 'dp', axis=0, tiled=True)  12.3 us
    all_gather x2, blocking collectives, on_device(): rows_all = lax.all_gather(mixed_here, 'dp', axis=0, tiled=True)  11.8 us
  transfers between devices with their start and end apart: 28, of which 25 were waited for; matrix products, arithmetic and copies ran while one was open for 22% of the time, Pallas kernels for 0%

profile of v1, /device:TPU:0, one launch (start us, length us, event | category | flops | bytes accessed | tf_op | source)
XLA Modules:
  0.0 396.1 jit_solution(9589916346645932603)
XLA Ops:
  7.2 6.9 %all_gather.18 = bf16[128,512]{1,0:T(8,128)(2,1)S(1)} all-gather(bf16[32,512]{1,0:T(8,128)(2,1)} %param.16), channel_id=1, replica_groups=mesh['tp'=8,'dp'=4] {'dp'}, dimensions={0}, use_global_device_ids=true | all-gather | bytes 163840 | tf_op jit(solution)/shard_map/all_gather | solution.py:83
  23.5 7.4 %collective-permute-done.1 = bf16[128,512]{1,0:T(8,128)(2,1)S(1)} collective-permute-done((bf16[128,512]{1,0:T(8,128)(2,1)S(1)}, bf16[128,512]{1,0:T(8,128)(2,1)S(1)}, u32[]{:S(2)}, u32[]{:S(2)}) %collective-permute-start.1) | collective-permute-done | bytes 131104 | tf_op jit(solution)/shard_map/ppermute | solution.py:86
  31.4 7.1 %collective-permute-done.2 = bf16[128,512]{1,0:T(8,128)(2,1)S(1)} collective-permute-done((bf16[128,512]{1,0:T(8,128)(2,1)S(1)}, bf16[128,512]{1,0:T(8,128)(2,1)S(1)}, u32[]{:S(2)}, u32[]{:S(2)}) %collective-permute-start.2) | collective-permute-done | bytes 131104 | tf_op jit(solution)/shard_map/ppermute | solution.py:86
  39.0 7.2 %collective-permute-done.3 = bf16[128,512]{1,0:T(8,128)(2,1)S(1)} collective-permute-done((bf16[128,512]{1,0:T(8,128)(2,1)S(1)}, bf16[128,512]{1,0:T(8,128)(2,1)S(1)}, u32[]{:S(2)}, u32[]{:S(2)}) %collective-permute-start.3) | collective-permute-done | bytes 131104 | tf_op jit(solution)/shard_map/ppermute | solution.py:86
  53.9 8.0 %collective-permute-done.5 = bf16[128,512]{1,0:T(8,128)(2,1)S(1)} collective-permute-done((bf16[128,512]{1,0:T(8,128)(2,1)S(1)}, bf16[128,512]{1,0:T(8,128)(2,1)S(1)}, u32[]{:S(2)}, u32[]{:S(2)}) %collective-permute-start.5) | collective-permute-done | bytes 131104 | tf_op jit(solution)/shard_map/ppermute | solution.py:86
  61.9 7.7 %collective-permute-done.6 = bf16[128,512]{1,0:T(8,128)(2,1)S(1)} collective-permute-done((bf16[128,512]{1,0:T(8,128)(2,1)S(1)}, bf16[128,512]{1,0:T(8,128)(2,1)S(1)}, u32[]{:S(2)}, u32[]{:S(2)}) %collective-permute-start.6) | collective-permute-done | bytes 131104 | tf_op jit(solution)/shard_map/ppermute | solution.py:86
  115.6 15.4 %fusion = f32[32,8,1,64]{3,2,1,0:T(1,128)S(1)} fusion(f32[32,8,64,1]{2,3,1,0:T(1,128)S(1)} %bitcast.154, f32[2,32,8,64,64]{4,3,2,1,0:T(8,128)} %param.29), kind=kOutput, calls=%fused_computation.2 | convolution fusion | flops 12582912 | bytes 8519680 | tf_op jit(solution)/shard_map/bhij,bhj->bhi/dot_general | solution.py:36
  131.0 11.1 %fusion.4 = f32[32,8,1,64]{3,2,1,0:T(1,128)S(1)} fusion(bf16[32,8,64,1]{2,3,1,0:T(2,128)(2,1)S(1)} %reshape.317, f32[2,32,8,64,64]{4,3,2,1,0:T(8,128)} %param.29, f32[32,8,64]{2,1,0:T(8,128)S(1)} %get-tuple-element.24, f32[32,8,64]{2,1,0:T(8,128)S(1)} %reshape.299, f32[32,8,64]{2,1,0:T(8,128)S(1)} %get-tuple-element.23, f32[32,8,64]{2,1,0:T(8,128)S(1)} %bitcast.150, ...), kind=kOutput, calls=%fused_computation.7 | convolution fusion | flops 18874368 | bytes 8814624 | tf_op jit(solution)/shard_map/bhij,bhj->bhi/dot_general | solution.py:43
  148.5 37.1 %all-gather.3.cloned.1.call-done = bf16[128,4096]{1,0:T(8,128)(2,1)} async-done(((bf16[128,512]{1,0:T(8,128)(2,1)}), bf16[128,4096]{1,0:T(8,128)(2,1)}) %all-gather.3.cloned.1.call-update) | async-done | bytes 1048592 | tf_op jit(solution)/shard_map/all_gather | solution.py:22
  187.6 6.6 %all_to_all.200 = bf16[4,32,128]{2,1,0:T(8,128)(2,1)S(1)} all-to-all(bf16[4,32,128]{2,1,0:T(8,128)(2,1)S(1)} %bitcast.159), channel_id=1, replica_groups=mesh['tp'=8,'dp'=4] {'dp'}, dimensions={0} | all-to-all | bytes 65536 | tf_op jit(solution)/shard_map/all_to_all | solution.py:129
  200.5 7.5 %collective-permute-done.7 = bf16[128,512]{1,0:T(8,128)(2,1)S(1)} collective-permute-done((bf16[128,512]{1,0:T(8,128)(2,1)S(1)}, bf16[128,512]{1,0:T(8,128)(2,1)S(1)}, u32[]{:S(2)}, u32[]{:S(2)}) %collective-permute-start.7) | collective-permute-done | bytes 131104 | tf_op jit(solution)/shard_map/ppermute | solution.py:86
  208.0 7.7 %collective-permute-done.8 = bf16[128,512]{1,0:T(8,128)(2,1)S(1)} collective-permute-done((bf16[128,512]{1,0:T(8,128)(2,1)S(1)}, bf16[128,512]{1,0:T(8,128)(2,1)S(1)}, u32[]{:S(2)}, u32[]{:S(2)}) %collective-permute-start.8) | collective-permute-done | bytes 131104 | tf_op jit(solution)/shard_map/ppermute | solution.py:86
  215.7 7.7 %collective-permute-done.9 = bf16[128,512]{1,0:T(8,128)(2,1)S(1)} collective-permute-done((bf16[128,512]{1,0:T(8,128)(2,1)S(1)}, bf16[128,512]{1,0:T(8,128)(2,1)S(1)}, u32[]{:S(2)}, u32[]{:S(2)}) %collective-permute-start.9) | collective-permute-done | bytes 131104 | tf_op jit(solution)/shard_map/ppermute | solution.py:86
  223.4 7.7 %collective-permute-done.10 = bf16[128,512]{1,0:T(8,128)(2,1)S(1)} collective-permute-done((bf16[128,512]{1,0:T(8,128)(2,1)S(1)}, bf16[128,512]{1,0:T(8,128)(2,1)S(1)}, u32[]{:S(2)}, u32[]{:S(2)}) %collective-permute-start.10) | collective-permute-done | bytes 131104 | tf_op jit(solution)/shard_map/ppermute | solution.py:86
  231.0 7.7 %collective-permute-done.11 = bf16[128,512]{1,0:T(8,128)(2,1)S(1)} collective-permute-done((bf16[128,512]{1,0:T(8,128)(2,1)S(1)}, bf16[128,512]{1,0:T(8,128)(2,1)S(1)}, u32[]{:S(2)}, u32[]{:S(2)}) %collective-permute-start.11) | collective-permute-done | bytes 131104 | tf_op jit(solution)/shard_map/ppermute | solution.py:86
  238.7 8.6 %collective-permute-done.12 = bf16[128,512]{1,0:T(8,128)(2,1)S(1)} collective-permute-done((bf16[128,512]{1,0:T(8,128)(2,1)S(1)}, bf16[128,512]{1,0:T(8,128)(2,1)S(1)}, u32[]{:S(2)}, u32[]{:S(2)}) %collective-permute-start.12) | collective-permute-done | bytes 131104 | tf_op jit(solution)/shard_map/ppermute | solution.py:86
  247.3 7.7 %collective-permute-done.13 = bf16[128,512]{1,0:T(8,128)(2,1)S(1)} collective-permute-done((bf16[128,512]{1,0:T(8,128)(2,1)S(1)}, bf16[128,512]{1,0:T(8,128)(2,1)S(1)}, u32[]{:S(2)}, u32[]{:S(2)}) %collective-permute-start.13) | collective-permute-done | bytes 131104 | tf_op jit(solution)/shard_map/ppermute | solution.py:86
  260.6 6.3 %all_to_all.201 = bf16[4,32,128]{2,1,0:T(8,128)(2,1)S(1)} all-to-all(bf16[4,32,128]{2,1,0:T(8,128)(2,1)S(1)} %bitcast.156), channel_id=1, replica_groups=mesh['tp'=8,'dp'=4] {'dp'}, dimensions={0} | all-to-all | bytes 65536 | tf_op jit(solution)/shard_map/all_to_all | solution.py:100
  300.0 15.4 %fusion.5 = f32[32,8,1,64]{3,2,1,0:T(1,128)S(1)} fusion(f32[32,8,64,1]{2,3,1,0:T(1,128)S(1)} %bitcast.155, f32[2,32,8,64,64]{4,3,2,1,0:T(8,128)} %param.29), kind=kOutput, calls=%fused_computation.9 | convolution fusion | flops 12582912 | bytes 8519680 | tf_op jit(solution)/shard_map/bhij,bhj->bhi/dot_general | solution.py:36
  315.5 11.1 %fusion.9 = f32[32,8,1,64]{3,2,1,0:T(1,128)S(1)} fusion(bf16[32,8,64,1]{2,3,1,0:T(2,128)(2,1)S(1)} %reshape.319, f32[2,32,8,64,64]{4,3,2,1,0:T(8,128)} %param.29, f32[32,8,64]{2,1,0:T(8,128)S(1)} %get-tuple-element.22, f32[32,8,64]{2,1,0:T(8,128)S(1)} %reshape.305, f32[32,8,64]{2,1,0:T(8,128)S(1)} %get-tuple-element.21, f32[32,8,64]{2,1,0:T(8,128)S(1)} %bitcast.152, ...), kind=kOutput, calls=%fused_computation.14 | convolution fusion | flops 18874368 | bytes 8814624 | tf_op jit(solution)/shard_map/bhij,bhj->bhi/dot_general | solution.py:43
  327.2 5.9 %all_gather.22 = bf16[128,512]{1,0:T(8,128)(2,1)} all-gather(bf16[32,512]{1,0:T(8,128)(2,1)S(1)} %fusion.59), channel_id=1, replica_groups=mesh['tp'=8,'dp'=4] {'dp'}, dimensions={0}, use_global_device_ids=true | all-gather | bytes 163840 | tf_op jit(solution)/shard_map/all_gather | solution.py:120
  333.1 13.7 %add_select_fusion.1 = (f32[1,32,8,64,64]{4,3,2,1,0:T(8,128)}, f32[1,32,8,64,64]{4,3,2,1,0:T(8,128)}) fusion(f32[2,32,8,64,64]{4,3,2,1,0:T(8,128)} %param.29, f32[32,8,64]{2,1,0:T(8,128)S(1)} %get-tuple-element.24, f32[32,8,64]{2,1,0:T(8,128)S(1)} %reshape.299, f32[32,8,64]{2,1,0:T(8,128)S(1)} %get-tuple-element.23, f32[32,8,64]{2,1,0:T(8,128)S(1)} %bitcast.151, ...), kind=kLoop, calls=%fused_computation.16 | loop fusion | flops 12582912 | bytes 17432608 | tf_op jit(solution)/shard_map/jit(_where)/select_n | solution.py:42
  346.8 23.5 %all-gather.5.cloned.1.call-done = bf16[128,4096]{1,0:T(8,128)(2,1)} async-done(((bf16[128,512]{1,0:T(8,128)(2,1)}), bf16[128,4096]{1,0:T(8,128)(2,1)}) %all-gather.5.cloned.1.call-update) | async-done | bytes 1048592 | tf_op jit(solution)/shard_map/all_gather | solution.py:22
  376.2 12.5 %pad_maximum_fusion = f32[2,32,8,64,64]{4,3,2,1,0:T(8,128)} fusion(f32[1,32,8,64,64]{4,3,2,1,0:T(8,128)} %get-tuple-element.8, f32[1,32,8,64,64]{4,3,2,1,0:T(8,128)} %get-tuple-element.7), kind=kLoop, calls=%fused_computation | loop fusion | flops 2097152 | bytes 16777216 | tf_op jit(solution)/shard_map/stack | solution.py:130
  (160 shorter events, 124.3 us)
Async XLA Ops:
  14.0 8.9 %collective-permute-start = (bf16[128,512]{1,0:T(8,128)(2,1)S(1)}, bf16[128,512]{1,0:T(8,128)(2,1)S(1)}, u32[]{:S(2)}, u32[]{:S(2)}) collective-permute-start(bf16[128,512]{1,0:T(8,128)(2,1)S(1)} %all_gather.18), channel_id=1, source_target_pairs={{0,4},{4,8},{8,12},{12,16},{16,20},{20,24},{24,28},{28,0},{1,5},{5... | collective-permute-start | bytes 393224 | tf_op jit(solution)/shard_map/ppermute | solution.py:86
  23.0 7.9 %collective-permute-start.1 = (bf16[128,512]{1,0:T(8,128)(2,1)S(1)}, bf16[128,512]{1,0:T(8,128)(2,1)S(1)}, u32[]{:S(2)}, u32[]{:S(2)}) collective-permute-start(bf16[128,512]{1,0:T(8,128)(2,1)S(1)} %collective-permute-done), channel_id=1, source_target_pairs={{0,4},{4,8},{8,12},{12,16},{16,20},{20,24},{24,28},{28,0},{1,5},{5... | collective-permute-start | bytes 393224 | tf_op jit(solution)/shard_map/ppermute | solution.py:86
  30.8 7.7 %collective-permute-start.2 = (bf16[128,512]{1,0:T(8,128)(2,1)S(1)}, bf16[128,512]{1,0:T(8,128)(2,1)S(1)}, u32[]{:S(2)}, u32[]{:S(2)}) collective-permute-start(bf16[128,512]{1,0:T(8,128)(2,1)S(1)} %collective-permute-done.1), channel_id=1, source_target_pairs={{0,4},{4,8},{8,12},{12,16},{16,20},{20,24},{24,28},{28,0},{1,5},{5... | collective-permute-start | bytes 393224 | tf_op jit(solution)/shard_map/ppermute | solution.py:86
  38.5 7.7 %collective-permute-start.3 = (bf16[128,512]{1,0:T(8,128)(2,1)S(1)}, bf16[128,512]{1,0:T(8,128)(2,1)S(1)}, u32[]{:S(2)}, u32[]{:S(2)}) collective-permute-start(bf16[128,512]{1,0:T(8,128)(2,1)S(1)} %collective-permute-done.2), channel_id=1, source_target_pairs={{0,4},{4,8},{8,12},{12,16},{16,20},{20,24},{24,28},{28,0},{1,5},{5... | collective-permute-start | bytes 393224 | tf_op jit(solution)/shard_map/ppermute | solution.py:86
  46.2 7.7 %collective-permute-start.4 = (bf16[128,512]{1,0:T(8,128)(2,1)S(1)}, bf16[128,512]{1,0:T(8,128)(2,1)S(1)}, u32[]{:S(2)}, u32[]{:S(2)}) collective-permute-start(bf16[128,512]{1,0:T(8,128)(2,1)S(1)} %collective-permute-done.3), channel_id=1, source_target_pairs={{0,4},{4,8},{8,12},{12,16},{16,20},{20,24},{24,28},{28,0},{1,5},{5... | collective-permute-start | bytes 393224 | tf_op jit(solution)/shard_map/ppermute | solution.py:86
  53.8 8.1 %collective-permute-start.5 = (bf16[128,512]{1,0:T(8,128)(2,1)S(1)}, bf16[128,512]{1,0:T(8,128)(2,1)S(1)}, u32[]{:S(2)}, u32[]{:S(2)}) collective-permute-start(bf16[128,512]{1,0:T(8,128)(2,1)S(1)} %collective-permute-done.4), channel_id=1, source_target_pairs={{0,4},{4,8},{8,12},{12,16},{16,20},{20,24},{24,28},{28,0},{1,5},{5... | collective-permute-start | bytes 393224 | tf_op jit(solution)/shard_map/ppermute | solution.py:86
  61.9 7.7 %collective-permute-start.6 = (bf16[128,512]{1,0:T(8,128)(2,1)S(1)}, bf16[128,512]{1,0:T(8,128)(2,1)S(1)}, u32[]{:S(2)}, u32[]{:S(2)}) collective-permute-start(bf16[128,512]{1,0:T(8,128)(2,1)S(1)} %collective-permute-done.5), channel_id=1, source_target_pairs={{0,4},{4,8},{8,12},{12,16},{16,20},{20,24},{24,28},{28,0},{1,5},{5... | collective-permute-start | bytes 393224 | tf_op jit(solution)/shard_map/ppermute | solution.py:86
  89.6 7.2 %all-to-all-start.2 = ((bf16[4,32,128]{2,1,0:T(8,128)(2,1)}), bf16[4,32,128]{2,1,0:T(8,128)(2,1)S(1)}, u32[]{:S(2)}, u32[]{:S(2)}) async-start(bf16[4,32,128]{2,1,0:T(8,128)(2,1)} %bitcast.17), calls=%async_computation.2 | async-start | bytes 65536 | tf_op jit(solution)/shard_map/all_to_all | solution.py:104
  103.9 7.2 %all-to-all-start = ((bf16[4,32,128]{2,1,0:T(8,128)(2,1)}), bf16[4,32,128]{2,1,0:T(8,128)(2,1)S(1)}, u32[]{:S(2)}, u32[]{:S(2)}) async-start(bf16[4,32,128]{2,1,0:T(8,128)(2,1)} %bitcast.9), calls=%async_computation | async-start | bytes 65536 | tf_op jit(solution)/shard_map/all_to_all | solution.py:103
  111.1 31.5 %all-to-all-start.5 = ((bf16[4,32,128]{2,1,0:T(8,128)(2,1)}), bf16[4,32,128]{2,1,0:T(8,128)(2,1)S(1)}, u32[]{:S(2)}, u32[]{:S(2)}) async-start(bf16[4,32,128]{2,1,0:T(8,128)(2,1)} %bitcast.26), calls=%async_computation.5 | async-start | bytes 65536 | tf_op jit(solution)/shard_map/all_to_all | solution.py:105
  114.4 71.2 %all-gather.3.cloned.1.call-start = ((), (), s32[]{:S(2)}) async-start(), calls=%async_computation.14 | async-start | bytes 1179648 | tf_op jit(solution)/shard_map/all_gather | solution.py:22
  199.6 8.4 %collective-permute-start.7 = (bf16[128,512]{1,0:T(8,128)(2,1)S(1)}, bf16[128,512]{1,0:T(8,128)(2,1)S(1)}, u32[]{:S(2)}, u32[]{:S(2)}) collective-permute-start(bf16[128,512]{1,0:T(8,128)(2,1)S(1)} %all_gather.21), channel_id=1, source_target_pairs={{0,4},{4,8},{8,12},{12,16},{16,20},{20,24},{24,28},{28,0},{1,5},{5... | collective-permute-start | bytes 393224 | tf_op jit(solution)/shard_map/ppermute | solution.py:86
  208.0 7.7 %collective-permute-start.8 = (bf16[128,512]{1,0:T(8,128)(2,1)S(1)}, bf16[128,512]{1,0:T(8,128)(2,1)S(1)}, u32[]{:S(2)}, u32[]{:S(2)}) collective-permute-start(bf16[128,512]{1,0:T(8,128)(2,1)S(1)} %collective-permute-done.7), channel_id=1, source_target_pairs={{0,4},{4,8},{8,12},{12,16},{16,20},{20,24},{24,28},{28,0},{1,5},{5... | collective-permute-start | bytes 393224 | tf_op jit(solution)/shard_map/ppermute | solution.py:86
  215.7 7.7 %collective-permute-start.9 = (bf16[128,512]{1,0:T(8,128)(2,1)S(1)}, bf16[128,512]{1,0:T(8,128)(2,1)S(1)}, u32[]{:S(2)}, u32[]{:S(2)}) collective-permute-start(bf16[128,512]{1,0:T(8,128)(2,1)S(1)} %collective-permute-done.8), channel_id=1, source_target_pairs={{0,4},{4,8},{8,12},{12,16},{16,20},{20,24},{24,28},{28,0},{1,5},{5... | collective-permute-start | bytes 393224 | tf_op jit(solution)/shard_map/ppermute | solution.py:86
  223.4 7.7 %collective-permute-start.10 = (bf16[128,512]{1,0:T(8,128)(2,1)S(1)}, bf16[128,512]{1,0:T(8,128)(2,1)S(1)}, u32[]{:S(2)}, u32[]{:S(2)}) collective-permute-start(bf16[128,512]{1,0:T(8,128)(2,1)S(1)} %collective-permute-done.9), channel_id=1, source_target_pairs={{0,4},{4,8},{8,12},{12,16},{16,20},{20,24},{24,28},{28,0},{1,5},{5... | collective-permute-start | bytes 393224 | tf_op jit(solution)/shard_map/ppermute | solution.py:86
  231.0 7.7 %collective-permute-start.11 = (bf16[128,512]{1,0:T(8,128)(2,1)S(1)}, bf16[128,512]{1,0:T(8,128)(2,1)S(1)}, u32[]{:S(2)}, u32[]{:S(2)}) collective-permute-start(bf16[128,512]{1,0:T(8,128)(2,1)S(1)} %collective-permute-done.10), channel_id=1, source_target_pairs={{0,4},{4,8},{8,12},{12,16},{16,20},{20,24},{24,28},{28,0},{1,5},{5... | collective-permute-start | bytes 393224 | tf_op jit(solution)/shard_map/ppermute | solution.py:86
  238.7 8.6 %collective-permute-start.12 = (bf16[128,512]{1,0:T(8,128)(2,1)S(1)}, bf16[128,512]{1,0:T(8,128)(2,1)S(1)}, u32[]{:S(2)}, u32[]{:S(2)}) collective-permute-start(bf16[128,512]{1,0:T(8,128)(2,1)S(1)} %collective-permute-done.11), channel_id=1, source_target_pairs={{0,4},{4,8},{8,12},{12,16},{16,20},{20,24},{24,28},{28,0},{1,5},{5... | collective-permute-start | bytes 393224 | tf_op jit(solution)/shard_map/ppermute | solution.py:86
  247.3 7.7 %collective-permute-start.13 = (bf16[128,512]{1,0:T(8,128)(2,1)S(1)}, bf16[128,512]{1,0:T(8,128)(2,1)S(1)}, u32[]{:S(2)}, u32[]{:S(2)}) collective-permute-start(bf16[128,512]{1,0:T(8,128)(2,1)S(1)} %collective-permute-done.12), channel_id=1, source_target_pairs={{0,4},{4,8},{8,12},{12,16},{16,20},{20,24},{24,28},{28,0},{1,5},{5... | collective-permute-start | bytes 393224 | tf_op jit(solution)/shard_map/ppermute | solution.py:86
  266.9 7.2 %all-to-all-start.8 = ((bf16[4,32,128]{2,1,0:T(8,128)(2,1)}), bf16[4,32,128]{2,1,0:T(8,128)(2,1)S(1)}, u32[]{:S(2)}, u32[]{:S(2)}) async-start(bf16[4,32,128]{2,1,0:T(8,128)(2,1)} %bitcast.40), calls=%async_computation.8 | async-start | bytes 65536 | tf_op jit(solution)/shard_map/all_to_all | solution.py:101
  274.0 7.4 %all-to-all-start.9 = ((bf16[4,32,128]{2,1,0:T(8,128)(2,1)}), bf16[4,32,128]{2,1,0:T(8,128)(2,1)S(1)}, u32[]{:S(2)}, u32[]{:S(2)}) async-start(bf16[4,32,128]{2,1,0:T(8,128)(2,1)} %bitcast.46), calls=%async_computation.9 | async-start | bytes 65536 | tf_op jit(solution)/shard_map/all_to_all | solution.py:104
  288.6 7.2 %all-to-all-start.7 = ((bf16[4,32,128]{2,1,0:T(8,128)(2,1)}), bf16[4,32,128]{2,1,0:T(8,128)(2,1)S(1)}, u32[]{:S(2)}, u32[]{:S(2)}) async-start(bf16[4,32,128]{2,1,0:T(8,128)(2,1)} %bitcast.38), calls=%async_computation.7 | async-start | bytes 65536 | tf_op jit(solution)/shard_map/all_to_all | solution.py:103
  295.8 31.3 %all-to-all-start.12 = ((bf16[4,32,128]{2,1,0:T(8,128)(2,1)}), bf16[4,32,128]{2,1,0:T(8,128)(2,1)S(1)}, u32[]{:S(2)}, u32[]{:S(2)}) async-start(bf16[4,32,128]{2,1,0:T(8,128)(2,1)} %bitcast.55), calls=%async_computation.12 | async-start | bytes 65536 | tf_op jit(solution)/shard_map/all_to_all | solution.py:105
  299.1 71.2 %all-gather.5.cloned.1.call-start = ((), (), s32[]{:S(2)}) async-start(), calls=%async_computation.15 | async-start | bytes 1179648 | tf_op jit(solution)/shard_map/all_gather | solution.py:22
  372.9 15.8 %all-to-all-start.13 = ((bf16[4,32,128]{2,1,0:T(8,128)(2,1)}), bf16[4,32,128]{2,1,0:T(8,128)(2,1)S(1)}, u32[]{:S(2)}, u32[]{:S(2)}) async-start(bf16[4,32,128]{2,1,0:T(8,128)(2,1)} %bitcast.58), calls=%async_computation.13 | async-start | bytes 65536 | tf_op jit(solution)/shard_map/all_to_all | solution.py:129
  (15 other events, 207.3 us)
Sparse Core Ops, SparseCore 0:
  148.7 36.9 all-gather.2
  333.2 37.0 all-gather.4
